TPU v7x, 32 devices: a whole 2x2x4 slice. The times are simulated.
32 devices in a mesh: ep: 8 (over z, x), tp: 4 (over y, core).
Axes of the slice: x: 2, y: 2, z: 4, core: 2. Of those that a mesh axis runs over, the one named last changes fastest.
Arguments:
- queries: bfloat16 [4096, 1024], P('ep', 'tp'), may hold values from -6 to 6
- forget_forward_logits: bfloat16 [4096, 1024], P('ep', 'tp'), may hold values from -6 to 12
- forget_backward_logits: bfloat16 [4096, 1024], P('ep', 'tp'), may hold values from -6 to 12
- values: bfloat16 [4096, 1024], P('ep', 'tp'), may hold values from -6 to 6
- output_gate_logits: bfloat16 [4096, 1024], P('ep', 'tp'), may hold values from -6 to 6
- lower_bound_forward: float32 [1024], P('tp')
- lower_bound_backward: float32 [1024], P('tp')
- extra_log_decay: float32 [4096, 8], P('ep', 'tp'), may hold values from -2 to 0
- head_norm_scale: float32 [1024], P('tp'), may hold values from 0.1 to 1.9
- output_projection: bfloat16 [1024, 2048], P('tp'), may hold values from -0.1875 to 0.1875
- second_residual: bfloat16 [4096, 2048], P('ep'), may hold values from -6 to 6
- expert_norm_scale: float32 [2048], replicated, may hold values from 0.1 to 1.9
- routes: int32 [4096, 2], P('ep'), may hold values from 0 to 7, all different within a row; in each aligned block of 128 rows (0 to 127, 128 to 255, ...) at most 64 rows name the same one
- specialist_mixing_factor: float32 [4096, 2], P(('ep', 'tp')), may hold values from 0.1 to 1
- expert_gate_matrix: bfloat16 [8, 2048, 1024], P('ep', None, 'tp'), may hold values from -0.125 to 0.125
- expert_up_matrix: bfloat16 [8, 2048, 1024], P('ep', None, 'tp'), may hold values from -0.125 to 0.125
- expert_down_matrix: bfloat16 [8, 1024, 2048], P('ep', 'tp'), may hold values from -0.1875 to 0.1875
Outputs:
- mixer_output: bfloat16 [4096, 2048], P(('ep', 'tp'))
- routed_output: bfloat16 [4096, 2048], P(('ep', 'tp'))
Inputs may be any that keep to these rules, and one draw needn't show every extreme that they name: `routes`: in each aligned block of 128 rows no expert is named by more than 64 rows; the 2 experts of a row differ.
All inputs are finite; a program needn't handle non-finite values.
Results may differ from a plain program's by a relative error of at most 0.014.
Values may be sent and summed in bfloat16 or wider, within the bound.
A program may use at most 128 MiB of HBM per device.

v0:
```python
import jax
import jax.numpy as jnp
from jax import lax
from jax.sharding import PartitionSpec as P

TOPK = 2
SPAN = 64


EPS = 1e-06
PRECISE_PRODUCT = lax.Precision.HIGHEST


def entering(shard, axis, join, neutral, backward):
    count = lax.axis_size(axis)
    place = lax.axis_index(axis)
    ahead = count - 1 - place if backward else place
    gathered = jax.tree.map(
        lambda a, kind: lax.all_gather(a.astype(kind), axis), shard, (jnp.bfloat16, jnp.bfloat16)
    )
    state = jax.tree.map(lambda a, e: jnp.zeros_like(a) + jnp.asarray(e, a.dtype), shard, neutral)

    def one(hop, state):
        source = count - 1 - hop if backward else hop
        return join(
            state,
            jax.tree.map(
                lambda a, own: lax.dynamic_index_in_dim(a, source, 0, False).astype(own.dtype),
                gathered,
                shard,
            ),
        )

    return lax.fori_loop(0, ahead, one, state)


def block_pass(feature, key_matrix_rows, value_rows, log_forget_decay):
    row_count, number_of_heads, channels = feature.shape
    blocks = row_count // SPAN
    lower_mask = jnp.tril(jnp.ones((SPAN, SPAN), bool))[:, :, None, None]

    def shaped(tensor):
        return tensor.reshape(blocks, SPAN, number_of_heads, tensor.shape[-1])

    def advance(progress, inputs):
        recurrent_memory, offset = progress
        query_tile_rows, address_piece_entries, content_piece_entries, decay_block = inputs
        progressive_summary = jnp.cumsum(decay_block, axis=0)
        spread_log = jnp.where(
            lower_mask, progressive_summary[:, None] - progressive_summary[None, :], -jnp.inf
        )
        scores = jnp.sum(
            query_tile_rows[:, None] * address_piece_entries[None, :] * jnp.exp(spread_log), axis=-1
        )
        inner_part = jnp.einsum(
            "tsh,shv->thv", scores, content_piece_entries, precision=PRECISE_PRODUCT
        )
        handed_summary = jnp.einsum(
            "wbf,bfl->wbl",
            query_tile_rows * jnp.exp(progressive_summary),
            recurrent_memory,
            precision=PRECISE_PRODUCT,
        )
        segment_fading_total = progressive_summary[-1]
        trained_portion = jnp.einsum(
            "gkf,gkr->kfr",
            address_piece_entries * jnp.exp(segment_fading_total[None] - progressive_summary),
            content_piece_entries,
            precision=PRECISE_PRODUCT,
        )
        recurrent_memory = (
            jnp.exp(segment_fading_total)[:, :, None] * recurrent_memory + trained_portion
        )
        return (
            (recurrent_memory, offset + segment_fading_total),
            (inner_part + handed_summary, query_tile_rows * jnp.exp(progressive_summary + offset)),
        )

    initial = (
        jnp.zeros((number_of_heads, channels, value_rows.shape[-1]), jnp.float32),
        jnp.zeros((number_of_heads, channels), jnp.float32),
    )
    (recurrent_memory, decay_total), (output_rows, query_decay_reach) = lax.scan(
        advance,
        initial,
        (shaped(feature), shaped(key_matrix_rows), shaped(value_rows), shaped(log_forget_decay)),
    )
    return (
        output_rows.reshape(row_count, number_of_heads, -1),
        query_decay_reach.reshape(row_count, number_of_heads, channels),
        recurrent_memory,
        decay_total,
    )


def forget_gate_terms(forget_gate_input, lower_bound_logit, extra_decay_rows, number_of_heads):
    row_count = forget_gate_input.shape[0]
    widened_values = forget_gate_input.astype(jnp.float32).reshape(row_count, number_of_heads, -1)
    lower_bound_share = jax.nn.sigmoid(lower_bound_logit).reshape(number_of_heads, -1)
    remaining_fraction = jax.nn.sigmoid(-lower_bound_logit).reshape(number_of_heads, -1)
    log_forget_decay = (
        jnp.log(lower_bound_share + remaining_fraction * jax.nn.sigmoid(widened_values))
        + extra_decay_rows[:, :, None]
    )
    return (remaining_fraction * jax.nn.sigmoid(-widened_values), log_forget_decay)


def finish_heads(combined, head_norm_scale, output_gate_logits, number_of_heads):
    mean_square = jnp.mean(combined * combined, axis=-1, keepdims=True)
    scaled = combined * lax.rsqrt(mean_square + EPS) * head_norm_scale.reshape(number_of_heads, -1)
    opened = scaled * jax.nn.silu(output_gate_logits.astype(jnp.float32)).reshape(combined.shape)
    return opened.astype(jnp.bfloat16).reshape(combined.shape[0], -1)


def normalize(tensor, gain):
    widened_values = tensor.astype(jnp.float32)
    return (
        widened_values
        * lax.rsqrt(jnp.mean(widened_values * widened_values, axis=-1, keepdims=True) + EPS)
        * gain
    ).astype(jnp.bfloat16)


def link_states(earlier, later_part):
    decay_early, memory_early = earlier
    decay_late, memory_late = later_part
    return (decay_early + decay_late, jnp.exp(decay_late)[:, :, None] * memory_early + memory_late)


def recurrent_half(
    queries,
    forget_forward_logits,
    forget_backward_logits,
    values,
    output_gate_logits,
    lower_bound_forward,
    lower_bound_backward,
    extra_log_decay,
    head_norm_scale,
    output_projection,
):
    row_count = queries.shape[0]
    number_of_heads = extra_log_decay.shape[1]
    feature = jax.nn.silu(queries.astype(jnp.float32)).reshape(row_count, number_of_heads, -1)
    value_rows = values.astype(jnp.float32).reshape(row_count, number_of_heads, -1)
    combined = jnp.zeros(value_rows.shape, jnp.float32)
    for forget_gate_input, lower_bound_logit, reverse in (
        (forget_forward_logits, lower_bound_forward, False),
        (forget_backward_logits, lower_bound_backward, True),
    ):
        key_matrix_rows, log_forget_decay = forget_gate_terms(
            forget_gate_input, lower_bound_logit, extra_log_decay, number_of_heads
        )
        if reverse:
            output_rows, query_decay_reach, recurrent_memory, decay_total = block_pass(
                jnp.flip(feature, 0),
                jnp.flip(key_matrix_rows, 0),
                jnp.flip(value_rows, 0),
                jnp.flip(log_forget_decay, 0),
            )
        else:
            output_rows, query_decay_reach, recurrent_memory, decay_total = block_pass(
                feature, key_matrix_rows, value_rows, log_forget_decay
            )
        identity = (jnp.zeros_like(decay_total), jnp.zeros_like(recurrent_memory))
        incoming_rows = entering(
            (decay_total, recurrent_memory), "ep", link_states, identity, reverse
        )
        output_rows = output_rows + jnp.einsum(
            "wbf,bfl->wbl", query_decay_reach, incoming_rows[1], precision=PRECISE_PRODUCT
        )
        if reverse:
            output_rows = jnp.flip(output_rows, 0)
        combined = combined + output_rows
    mixer_hidden = finish_heads(combined, head_norm_scale, output_gate_logits, number_of_heads)
    return lax.psum_scatter(
        jnp.dot(mixer_hidden, output_projection, preferred_element_type=jnp.float32).astype(
            jnp.bfloat16
        ),
        "tp",
        scatter_dimension=0,
        tiled=True,
    )


def expert_hidden(rows_in, expert_gate_matrix, expert_up_matrix):
    gated = jnp.dot(rows_in, expert_gate_matrix[0], preferred_element_type=jnp.float32)
    lifted = jnp.dot(rows_in, expert_up_matrix[0], preferred_element_type=jnp.float32)
    return (jax.nn.silu(gated) * lifted).astype(jnp.bfloat16)


def routed_half(
    second_residual,
    expert_norm_scale,
    routes,
    specialist_mixing_factor,
    expert_gate_matrix,
    expert_up_matrix,
    expert_down_matrix,
):
    group_rows, width_model = second_residual.shape
    quarters = lax.axis_size("tp")
    experts = lax.axis_size("ep")
    row_count = group_rows // quarters
    slot_count = 2 * TOPK * row_count // experts
    quarter = lax.axis_index("tp")
    own_rows = normalize(
        lax.dynamic_slice_in_dim(second_residual, quarter * row_count, row_count, 0),
        expert_norm_scale,
    )
    flat_routes = lax.dynamic_slice_in_dim(routes, quarter * row_count, row_count, 0).reshape(-1)
    expert_hits = (flat_routes[:, None] == jnp.arange(experts, dtype=jnp.int32)[None, :]).astype(
        jnp.int32
    )
    ranking = jnp.sum(jnp.cumsum(expert_hits, axis=0) * expert_hits, axis=1) - 1
    target = flat_routes * slot_count + ranking
    own_pick = (
        target[:, None] == jnp.arange(experts * slot_count, dtype=jnp.int32)[None, :]
    ).astype(jnp.bfloat16)
    chooser = own_pick.reshape(row_count, TOPK, -1).sum(axis=1)
    outgoing = jnp.einsum(
        "rs,rd->sd", chooser, own_rows, preferred_element_type=jnp.float32
    ).astype(jnp.bfloat16)
    arrived = lax.all_to_all(
        outgoing.reshape(experts, slot_count, width_model),
        "ep",
        split_axis=0,
        concat_axis=0,
        tiled=True,
    )
    hidden = expert_hidden(
        lax.all_gather(arrived.reshape(-1, width_model), "tp", axis=0, tiled=True),
        expert_gate_matrix,
        expert_up_matrix,
    )
    summed = lax.psum_scatter(
        jnp.dot(hidden, expert_down_matrix[0], preferred_element_type=jnp.float32).astype(
            jnp.bfloat16
        ),
        "tp",
        scatter_dimension=0,
        tiled=True,
    )
    returned = lax.all_to_all(
        summed.reshape(experts, slot_count, width_model),
        "ep",
        split_axis=0,
        concat_axis=0,
        tiled=True,
    )
    gathered = jnp.dot(
        own_pick, returned.reshape(-1, width_model), preferred_element_type=jnp.float32
    )
    blended = jnp.sum(
        gathered.reshape(row_count, TOPK, width_model) * specialist_mixing_factor[:, :, None],
        axis=1,
    )
    return blended.astype(jnp.bfloat16)


def shards(
    queries,
    forget_forward_logits,
    forget_backward_logits,
    values,
    output_gate_logits,
    lower_bound_forward,
    lower_bound_backward,
    extra_log_decay,
    head_norm_scale,
    output_projection,
    second_residual,
    expert_norm_scale,
    routes,
    specialist_mixing_factor,
    expert_gate_matrix,
    expert_up_matrix,
    expert_down_matrix,
):
    mixer_output = recurrent_half(
        queries,
        forget_forward_logits,
        forget_backward_logits,
        values,
        output_gate_logits,
        lower_bound_forward,
        lower_bound_backward,
        extra_log_decay,
        head_norm_scale,
        output_projection,
    )
    routed_output = routed_half(
        second_residual,
        expert_norm_scale,
        routes,
        specialist_mixing_factor,
        expert_gate_matrix,
        expert_up_matrix,
        expert_down_matrix,
    )
    return (mixer_output, routed_output)


def solution(mesh):
    in_specs = (
        P("ep", "tp"),
        P("ep", "tp"),
        P("ep", "tp"),
        P("ep", "tp"),
        P("ep", "tp"),
        P("tp"),
        P("tp"),
        P("ep", "tp"),
        P("tp"),
        P("tp", None),
        P("ep", None),
        P(),
        P("ep", None),
        P(("ep", "tp"), None),
        P("ep", None, "tp"),
        P("ep", None, "tp"),
        P("ep", "tp", None),
    )
    out_specs = (P(("ep", "tp"), None), P(("ep", "tp"), None))
    return jax.shard_map(shards, mesh=mesh, in_specs=in_specs, out_specs=out_specs, check_vma=False)
```

profile of v0, /device:TPU:0, one launch (start us, length us, event | category | flops | bytes accessed | tf_op | source)
XLA Modules:
  0.0 400.6 jit_solution(1983032808302991070)
XLA Ops:
  11.6 3.2 convolution_convert_fusion.1
  14.8 7.4 %all-to-all-start = ((bf16[8,64,2048]{2,1,0:T(8,128)(2,1)}), bf16[8,64,2048]{2,1,0:T(8,128)(2,1)S(1)}, u32[]{:S(2)}, u32[]{:S(2)}) async-start(bf16[8,64,2048]{2,1,0:T(8,128)(2,1)} %bitcast.30), calls=%async_computation.1 | async-start | bytes 4194304 | tf_op jit(solution)/shard_map/all_to_all | solution.py:224
  22.3 1.9 convert_multiply_fusion.3
  24.2 2.1 reshape.248
  26.3 2.1 reshape_reshape.7
  32.0 2.2 reshape.272
  35.0 2.0 rev.19
  37.1 5.0 %rev.18 = f32[512,2,128]{0,2,1:T(8,128)} reverse(f32[512,2,128]{0,2,1:T(8,128)} %bitcast.232), dimensions={0} | reverse | bytes 1048576 | tf_op jit(solution)/shard_map/jit(_flip)/rev | solution.py:158
  42.1 2.0 copy.155
  46.0 2.0 copy.162
  48.1 2.4 copy.149
  50.4 2.2 fusion.74
  52.6 2.1 div.66
  54.8 2.1 div.64
  56.9 2.7 broadcast_multiply_fusion.1
  59.6 10.9 %all-to-all-done = bf16[8,64,2048]{2,1,0:T(8,128)(2,1)S(1)} async-done(((bf16[8,64,2048]{2,1,0:T(8,128)(2,1)}), bf16[8,64,2048]{2,1,0:T(8,128)(2,1)S(1)}, u32[]{:S(2)}, u32[]{:S(2)}) %all-to-all-start) | async-done | bytes 2097184 | tf_op jit(solution)/shard_map/all_to_all | solution.py:224
  72.3 59.4 %while.62 = (s32[]{:T(128)}, f32[2,128,128]{2,1,0:T(8,128)S(1)}, f32[2,128]{1,0:T(2,128)S(1)}, f32[8,64,2,128]{3,1,0,2:T(8,128)S(1)}, f32[8,64,2,128]{3,2,1,0:T(...) while((s32[]{:T(128)}, f32[2,128,128]{2,1,0:T(8,128)S(1)}, ...), condition=%wide.region_3.4_spmd.clone, body=%wide.region_0.3_spmd.clone.sunk | while | flops 69415424 | bytes 2246809 | solution.py:83
  74.3 2.0 multiply_reduce_fusion.5
  81.8 2.0 multiply_reduce_fusion.5
  89.2 2.0 multiply_reduce_fusion.5
  96.6 2.0 multiply_reduce_fusion.5
  104.0 2.0 multiply_reduce_fusion.5
  111.5 2.0 multiply_reduce_fusion.5
  118.9 2.0 multiply_reduce_fusion.5
  126.3 2.0 multiply_reduce_fusion.5
  133.1 2.1 div.73
  136.2 2.5 broadcast_multiply_fusion
  138.7 2.0 rev.17
  141.7 7.3 %fusion.67 = f32[2048,256]{1,0:T(8,128)} fusion(bf16[2048,2048]{1,0:T(8,128)(2,1)} %all-gather.8.cloned.1.call-done, bf16[1,2048,256]{2,1,0:T(8,128)(2,1)} %param.39), kind=kOutput, calls=%fused_computation.101 | convolution fusion | flops 2147483648 | bytes 11534336 | tf_op jit(solution)/shard_map/dot_general | solution.py:187
  149.1 16.8 %convolution_convert_fusion = bf16[2048,2048]{1,0:T(8,128)(2,1)} fusion(bf16[2048,2048]{1,0:T(8,128)(2,1)} %all-gather.8.cloned.1.call-done, f32[2048,256]{1,0:T(8,128)} %fusion.67, bf16[1,256,2048]{2,1,0:T(8,128)(2,1)S(1)} %copy-done, bf16[1,2048,256]{2,1,0:T(8,128)(2,1)} %param.40), kind=kOutput, calls=%fused_computation.82 | convolution fusion | flops 4302307328 | bytes 20971520 | tf_op jit(solution)/shard_map/dot_general | solution.py:237
  167.2 64.6 %while.63 = (s32[]{:T(128)}, f32[2,128,128]{2,1,0:T(8,128)S(1)}, f32[2,128]{1,0:T(2,128)S(1)}, f32[8,64,2,128]{3,1,0,2:T(8,128)}, f32[8,64,2,128]{3,2,1,0:T(2,12...) while((s32[]{:T(128)}, f32[2,128,128]{2,1,0:T(8,128)S(1)}, ...), condition=%wide.region_9.10_spmd.clone, body=%wide.region_6.9_spmd.clone.sunk | while | flops 69415424 | bytes 2246809 | solution.py:83
  169.1 2.0 multiply_reduce_fusion.6
  177.3 2.0 multiply_reduce_fusion.6
  185.4 2.0 multiply_reduce_fusion.6
  193.4 2.0 multiply_reduce_fusion.6
  201.5 2.0 multiply_reduce_fusion.6
  209.6 2.0 multiply_reduce_fusion.6
  217.7 2.0 multiply_reduce_fusion.6
  225.7 2.0 multiply_reduce_fusion.6
  233.9 18.6 %all-gather.5 = bf16[8,2,128]{2,1,0:T(2,128)(2,1)S(1)} all-gather(bf16[1,2,128]{2,1,0:T(2,128)(2,1)S(1)} %convert_bitcast_fusion), channel_id=4, replica_groups=mesh['ep'=8,'tp'=4] {'ep'}, dimensions={0}, use_global_device_ids=true | all-gather | bytes 4608 | tf_op jit(solution)/shard_map/all_gather | solution.py:19
  252.5 33.5 %all-gather.3 = bf16[16,128,128]{2,1,0:T(8,128)(2,1)} all-gather(bf16[2,128,128]{2,1,0:T(8,128)(2,1)S(1)} %convert_element_type.107), channel_id=5, replica_groups=mesh['ep'=8,'tp'=4] {'ep'}, dimensions={0}, use_global_device_ids=true | all-gather | bytes 589824 | tf_op jit(solution)/shard_map/all_gather | solution.py:19
  286.0 7.1 %while.61 = (s32[]{:T(128)}, f32[2,128,128]{2,1,0:T(8,128)S(1)}, s32[]{:T(128)}, bf16[8,2,128]{2,1,0:T(2,128)(2,1)S(1)}, bf16[8,2,128,128]{3,2,1,0:T(8,128)(2,1)...) while((s32[]{:T(128)}, f32[2,128,128]{2,1,0:T(8,128)S(1)}, s32[]{:T(128)}, ...), condition=%wide.region_11.12_spmd, body=%wide.region_10.11_spmd.sunk | while | flops 98566 | bytes 330395 | solution.py:34
  293.1 2.5 fusion.60
  295.6 3.8 rev.20
  299.4 16.3 %all-gather.4 = bf16[8,2,128]{2,1,0:T(2,128)(2,1)S(1)} all-gather(bf16[1,2,128]{2,1,0:T(2,128)(2,1)S(1)} %convert_bitcast_fusion.1), channel_id=2, replica_groups=mesh['ep'=8,'tp'=4] {'ep'}, dimensions={0}, use_global_device_ids=true | all-gather | bytes 4608 | tf_op jit(solution)/shard_map/all_gather | solution.py:19
  315.7 33.5 %all-gather.1 = bf16[16,128,128]{2,1,0:T(8,128)(2,1)} all-gather(bf16[2,128,128]{2,1,0:T(8,128)(2,1)S(1)} %convert_element_type.104), channel_id=3, replica_groups=mesh['ep'=8,'tp'=4] {'ep'}, dimensions={0}, use_global_device_ids=true | all-gather | bytes 589824 | tf_op jit(solution)/shard_map/all_gather | solution.py:19
  351.1 2.0 convolution_convert_fusion.2
  353.2 39.2 %all_to_all.10 = bf16[8,64,2048]{2,1,0:T(8,128)(2,1)S(1)} all-to-all(bf16[8,64,2048]{2,1,0:T(8,128)(2,1)} %bitcast.229), channel_id=1, replica_groups=mesh['ep'=8,'tp'=4] {'ep'}, dimensions={0} | all-to-all | bytes 4194304 | tf_op jit(solution)/shard_map/all_to_all | solution.py:244
  (268 shorter events, 121.0 us)
Async XLA Ops:
  7.2 141.9 %copy-start = (bf16[1,256,2048]{2,1,0:T(8,128)(2,1)S(1)}, bf16[1,256,2048]{2,1,0:T(8,128)(2,1)}, u32[]{:S(2)}) copy-start(bf16[1,256,2048]{2,1,0:T(8,128)(2,1)} %param.41) | copy-start | bytes 3145732
  14.8 19.3 %copy-start.6 = (f32[512,2]{0,1:T(2,128)S(1)}, f32[512,2]{0,1:T(2,128)}, u32[]{:S(2)}) copy-start(f32[512,2]{0,1:T(2,128)} %param.32) | copy-start | bytes 12292
  14.8 55.7 %all-to-all-start = ((bf16[8,64,2048]{2,1,0:T(8,128)(2,1)}), bf16[8,64,2048]{2,1,0:T(8,128)(2,1)S(1)}, u32[]{:S(2)}, u32[]{:S(2)}) async-start(bf16[8,64,2048]{2,1,0:T(8,128)(2,1)} %bitcast.30), calls=%async_computation.1 | async-start | bytes 4194304 | tf_op jit(solution)/shard_map/all_to_all | solution.py:224
  22.2 119.5 %all-gather.8.cloned.1.call-start = ((), (), s32[]{:S(2)}) async-start(), calls=%async_computation.5 | async-start | bytes 10485760 | tf_op jit(solution)/shard_map/all_gather | solution.py:232
  42.1 14.8 %copy-start.7 = (f32[256]{0:T(256)S(1)}, f32[256]{0:T(256)}, u32[]{:S(2)}) copy-start(f32[256]{0:T(256)} %param.30) | copy-start | bytes 3076
  70.5 1.4 copy-start.1
  71.8 281.4 %reduce-scatter.5.cloned.1.call-start = ((), (), s32[]{:S(2)}) async-start(), calls=%async_computation.6 | async-start | bytes 10485760 | tf_op jit(solution)/shard_map/reduce_scatter | solution.py:236
  72.3 59.7 %copy-start.5 = (bf16[512,256]{1,0:T(8,128)(2,1)S(1)}, bf16[512,256]{1,0:T(8,128)(2,1)}, u32[]{:S(2)}) copy-start(bf16[512,256]{1,0:T(8,128)(2,1)} %param.27) | copy-start | bytes 786436
  131.7 4.5 %copy-start.8 = (f32[256]{0:T(256)S(1)}, f32[256]{0:T(256)}, u32[]{:S(2)}) copy-start(f32[256]{0:T(256)} %param.31) | copy-start | bytes 3076
  131.7 4.5 %copy-start.2 = (f32[512,2]{1,0:T(8,128)S(1)}, f32[512,2]{1,0:T(8,128)}, u32[]{:S(2)}) copy-start(f32[512,2]{1,0:T(8,128)} %copy.168) | copy-start | bytes 12292
  165.9 228.1 %reduce-scatter.3.cloned.1.call-start = ((), (), s32[]{:S(2)}) async-start(), calls=%async_computation.4 | async-start | bytes 2621440 | tf_op jit(solution)/shard_map/reduce_scatter | solution.py:176
  231.8 0.8 copy-start.3
  293.1 56.9 %copy-start.9 = (f32[256]{0:T(256)S(1)}, f32[256]{0:T(256)}, u32[]{:S(2)}) copy-start(f32[256]{0:T(256)} %param.33) | copy-start | bytes 3076
  349.2 1.9 copy-start.4
  353.2 39.2 %copy-start.10 = (f32[128,2]{0,1:T(2,128)S(1)}, f32[128,2]{0,1:T(2,128)}, u32[]{:S(2)}) copy-start(f32[128,2]{0,1:T(2,128)} %param.38) | copy-start | bytes 3076
Sparse Core Ops, SparseCore 0:
  72.0 57.3 all-gather.7
  166.0 70.5 reduce-scatter.4
  353.3 37.0 reduce-scatter.2
where the time goes:
time: 406 us; the launch traced here: 401 us
  blocking collectives  141 us (35%)
  other arithmetic  102 us (25%)
  matrix products  79.8 us (20%)
  local copies, waits for them, and re-layouts  43.3 us (11%)
  between operations  14.1 us (3%)
  waiting for transfers between devices  11 us (3%)
  starting transfers between devices  7.93 us (2%)
    all_gather x4, blocking collectives, entering(): lax.all_gather(a.astype(kind), axis)  102 us
    all_to_all x1, blocking collectives, routed_half(): lax.all_to_all(summed.reshape(experts, slot_count, width_model), 'ep', sp...  39.2 us
    reduce_sum x16, other arithmetic, advance(): jnp.sum(query_tile_rows[:, None] * address_piece_entries[None, :] * jnp.e...  31.6 us
    dot_general x16, matrix products, advance(): jnp.einsum('gkf,gkr->kfr', address_piece_entries * jnp.exp(segment_fading...  19.8 us
    dot_general x1, matrix products, routed_half(): jnp.dot(hidden, expert_down_matrix[0], preferred_element_type=jnp.float32)  16.8 us
    dot_general x16, matrix products, advance(): jnp.einsum('tsh,shv->thv', scores, content_piece_entries, precision=PRECI...  16.8 us
    mul x16, other arithmetic, advance(): query_tile_rows * jnp.exp(progressive_summary)  15.9 us
    another operation x16, other arithmetic, advance(): progressive_summary = jnp.cumsum(decay_block, axis=0)  14.7 us
  transfers between devices with their start and end apart: 4, of which 1 were waited for; matrix products, arithmetic and copies ran while one was open for 48% of the time, Pallas kernels for 0%

commit v1 on v0

v1 whole, which is shorter than its diff:
```python
import functools

import jax
import jax.numpy as jnp
from jax import lax
from jax.experimental import pallas as pl
from jax.experimental.pallas import tpu as pltpu
from jax.sharding import PartitionSpec as P

TOPK = 2
CHUNK = 128
LEAF = 16
DECAY_ROWS = 16
EPS = 1e-06
MESH = pl.DeviceIdType.MESH
F32 = jnp.float32
BF16 = jnp.bfloat16


def greet(n):
    me = lax.axis_index("ep")
    barrier = pltpu.get_barrier_semaphore()

    def one(step, carry):
        peer = lax.rem(me + step, n)
        pl.semaphore_signal(barrier, inc=1, device_id={"ep": peer}, device_id_type=MESH)
        return carry

    lax.fori_loop(1, n, one, 0)
    pl.semaphore_wait(barrier, n - 1)


def block_copy(out_ref, in_ref, send_sem, recv_sem, target, source):
    me = lax.axis_index("ep")
    return pltpu.make_async_remote_copy(
        src_ref=out_ref.at[target],
        dst_ref=in_ref.at[source],
        send_sem=send_sem.at[target],
        recv_sem=recv_sem.at[source],
        device_id={"ep": target},
        device_id_type=MESH,
    )


def start_blocks(n, out_ref, in_ref, send_sem, recv_sem):
    me = lax.axis_index("ep")

    def one(step, carry):
        peer = lax.rem(me + step, n)
        block_copy(out_ref, in_ref, send_sem, recv_sem, peer, me).start()
        return carry

    lax.fori_loop(1, n, one, 0)
    in_ref[me] = out_ref[me]


def finish_blocks(n, out_ref, in_ref, send_sem, recv_sem):
    me = lax.axis_index("ep")

    def one(step, carry):
        peer = lax.rem(me + step, n)
        copy = block_copy(out_ref, in_ref, send_sem, recv_sem, peer, peer)
        copy.wait_send()
        copy.wait_recv()
        return carry

    lax.fori_loop(1, n, one, 0)


def exchange_kernel(n, out_ref, in_ref, send_sem, recv_sem):
    greet(n)
    start_blocks(n, out_ref, in_ref, send_sem, recv_sem)
    finish_blocks(n, out_ref, in_ref, send_sem, recv_sem)


def exchange(blocks, n):
    vmem = pl.BlockSpec(memory_space=pltpu.VMEM)
    return pl.pallas_call(
        functools.partial(exchange_kernel, n),
        out_shape=jax.ShapeDtypeStruct(blocks.shape, blocks.dtype),
        in_specs=[vmem],
        out_specs=vmem,
        scratch_shapes=[pltpu.SemaphoreType.DMA((n,)), pltpu.SemaphoreType.DMA((n,))],
        compiler_params=pltpu.CompilerParams(collective_id=1, has_side_effects=True),
        cost_estimate=pl.CostEstimate(
            flops=2 * 10**10, bytes_accessed=2 * blocks.size * 2, transcendentals=0
        ),
        name="return_rows",
    )(blocks)


def dot_rows(a, b):
    return lax.dot_general(a, b, (((1,), (1,)), ((), ())), preferred_element_type=F32)


def gates(logits, bound, extra):
    shrink = jnp.exp(-logits)
    opened = 1.0 / (1.0 + shrink)
    floor_part = 1.0 / (1.0 + jnp.exp(-bound))
    complement = 1.0 / (1.0 + jnp.exp(bound))
    decay = jnp.log(floor_part + complement * opened) + extra
    return complement * (shrink * opened), decay


def referenced(total, size, place):
    blocks = total.reshape(CHUNK // size, size, total.shape[-1])
    anchor = jnp.broadcast_to(blocks[:, place : place + 1, :], blocks.shape)
    return total - anchor.reshape(total.shape)


def chunk_scores(feature, key, total, backward, rows, cols):
    scores = jnp.zeros((CHUNK, CHUNK), F32)
    size = CHUNK
    while size > LEAF:
        half = size // 2
        reach = jnp.exp(-jnp.abs(referenced(total, size, half if backward else half - 1)))
        part = dot_rows((feature * reach).astype(BF16), (key * reach).astype(BF16))
        late, early = (cols, rows) if backward else (rows, cols)
        mask = (rows // size == cols // size) & (late % size >= half) & (early % size < half)
        scores = scores + jnp.where(mask, part, 0.0)
        size = half
    spread = referenced(total, LEAF, LEAF // 2 if backward else LEAF // 2 - 1)
    part = dot_rows(
        (feature * jnp.exp(spread)).astype(BF16), (key * jnp.exp(-spread)).astype(BF16)
    )
    mask = (rows // LEAF == cols // LEAF) & ((rows <= cols) if backward else (rows >= cols))
    return scores + jnp.where(mask, part, 0.0)


def mixer_kernel(
    n,
    q_ref,
    ff_ref,
    fb_ref,
    v_ref,
    og_ref,
    lbf_ref,
    lbb_ref,
    extra_ref,
    scale_ref,
    slots_ref,
    hidden_ref,
    arrived_ref,
    local_ref,
    reach_ref,
    part_ref,
    fade_ref,
    state_out,
    state_in,
    slot_send,
    slot_recv,
    state_send,
    state_recv,
):
    me = lax.axis_index("ep")
    row_count, width = q_ref.shape
    chunks = row_count // CHUNK
    heads = extra_ref.shape[1]
    channels = width // heads
    greet(n)
    start_blocks(n, slots_ref, arrived_ref, slot_send, slot_recv)
    rows = lax.broadcasted_iota(jnp.int32, (CHUNK, CHUNK), 0)
    cols = lax.broadcasted_iota(jnp.int32, (CHUNK, CHUNK), 1)

    def local(c, carry):
        at = pl.ds(pl.multiple_of(c * CHUNK, CHUNK), CHUNK)
        for h in range(heads):
            lanes = slice(h * channels, (h + 1) * channels)
            queries = q_ref[at, lanes].astype(F32)
            feature = queries / (1.0 + jnp.exp(-queries))
            value_rows = v_ref[at, lanes]
            extra = extra_ref[at, h : h + 1]
            scores = jnp.zeros((CHUNK, CHUNK), F32)
            for way, (logit_ref, bound_ref) in enumerate(((ff_ref, lbf_ref), (fb_ref, lbb_ref))):
                key, decay = gates(logit_ref[at, lanes].astype(F32), bound_ref[:, lanes], extra)
                order = (rows <= cols) if way else (rows >= cols)
                total = jnp.dot(
                    order.astype(F32),
                    decay,
                    preferred_element_type=F32,
                    precision=lax.Precision.HIGHEST,
                )
                edge = total[0:1] if way else total[CHUNK - 1 : CHUNK]
                scores = scores + chunk_scores(feature, key, total, way == 1, rows, cols)
                reach_ref[way, h, c] = (feature * jnp.exp(total)).astype(BF16)
                faded = (key * jnp.exp(edge - total)).astype(BF16)
                part_ref[way, h, c] = lax.dot_general(
                    value_rows, faded, (((0,), (0,)), ((), ())), preferred_element_type=F32
                )
                fade_ref[way, h, c] = jnp.broadcast_to(jnp.exp(edge), (8, channels))
            local_ref[h, c] = jnp.dot(
                scores.astype(BF16), value_rows, preferred_element_type=F32
            )
        return carry

    lax.fori_loop(0, chunks, local, 0)
    for way in range(2):
        for h in range(heads):
            state = jnp.zeros(part_ref.shape[3:], F32)
            fade = jnp.ones((1, channels), F32)
            for c in range(chunks)[:: -1 if way else 1]:
                step = fade_ref[way, h, c, 0:1]
                state = state * step + part_ref[way, h, c]
                fade = fade * step
            state_out[way, h, : state.shape[0]] = state.astype(BF16)
            state_out[way, h, state.shape[0] :] = jnp.broadcast_to(
                fade, (DECAY_ROWS, channels)
            ).astype(BF16)

    def state_copy(target, source):
        way = jnp.where(target > me, 0, 1)
        return pltpu.make_async_remote_copy(
            src_ref=state_out.at[way],
            dst_ref=state_in.at[source],
            send_sem=state_send.at[target],
            recv_sem=state_recv.at[source],
            device_id={"ep": target},
            device_id_type=MESH,
        )

    def send(step, carry):
        state_copy(lax.rem(me + step, n), me).start()
        return carry

    def receive(step, carry):
        peer = lax.rem(me + step, n)
        copy = state_copy(peer, peer)
        copy.wait_send()
        copy.wait_recv()
        return carry

    lax.fori_loop(1, n, send, 0)
    lax.fori_loop(1, n, receive, 0)
    depth = part_ref.shape[3]
    for h in range(heads):
        for way in range(2):

            def one(hop, state, way=way, h=h):
                source = n - 1 - hop if way else hop
                step = state_in[source, h, depth : depth + DECAY_ROWS].astype(F32)[0:1]
                return state * step + state_in[source, h, :depth].astype(F32)

            ahead = n - 1 - me if way else me
            state = lax.fori_loop(0, ahead, one, jnp.zeros(part_ref.shape[3:], F32))
            for c in range(chunks)[:: -1 if way else 1]:
                local_ref[h, c] += dot_rows(reach_ref[way, h, c], state.astype(BF16))
                state = state * fade_ref[way, h, c, 0:1] + part_ref[way, h, c]
        lanes = slice(h * channels, (h + 1) * channels)
        for c in range(chunks):
            at = slice(c * CHUNK, (c + 1) * CHUNK)
            combined = local_ref[h, c]
            mean_square = jnp.mean(combined * combined, axis=-1, keepdims=True)
            gate = og_ref[at, lanes].astype(F32)
            opened = combined * lax.rsqrt(mean_square + EPS) * scale_ref[:, lanes]
            hidden_ref[at, lanes] = (opened * (gate / (1.0 + jnp.exp(-gate)))).astype(BF16)
    finish_blocks(n, slots_ref, arrived_ref, slot_send, slot_recv)


def mixer(n, queries, ff, fb, values, og, lbf, lbb, extra, scale, slots):
    row_count, width = queries.shape
    heads = extra.shape[1]
    channels = width // heads
    depth = values.shape[1] // heads
    chunks = row_count // CHUNK
    vmem = pl.BlockSpec(memory_space=pltpu.VMEM)
    state = (heads, depth + DECAY_ROWS, channels)
    return pl.pallas_call(
        functools.partial(mixer_kernel, n),
        out_shape=(
            jax.ShapeDtypeStruct(values.shape, BF16),
            jax.ShapeDtypeStruct(slots.shape, slots.dtype),
        ),
        in_specs=[vmem] * 10,
        out_specs=(vmem, vmem),
        scratch_shapes=[
            pltpu.VMEM((heads, chunks, CHUNK, depth), F32),
            pltpu.VMEM((2, heads, chunks, CHUNK, channels), BF16),
            pltpu.VMEM((2, heads, chunks, depth, channels), F32),
            pltpu.VMEM((2, heads, chunks, 8, channels), F32),
            pltpu.VMEM((2,) + state, BF16),
            pltpu.VMEM((n,) + state, BF16),
            pltpu.SemaphoreType.DMA((n,)),
            pltpu.SemaphoreType.DMA((n,)),
            pltpu.SemaphoreType.DMA((n,)),
            pltpu.SemaphoreType.DMA((n,)),
        ],
        compiler_params=pltpu.CompilerParams(
            collective_id=0, has_side_effects=True, vmem_limit_bytes=48 * 2**20
        ),
        cost_estimate=pl.CostEstimate(
            flops=4 * 10**10, bytes_accessed=6 * 2**20, transcendentals=0
        ),
        name="mix_dispatch",
    )(
        queries,
        ff,
        fb,
        values,
        og,
        lbf.reshape(1, -1),
        lbb.reshape(1, -1),
        extra,
        scale.reshape(1, -1),
        slots,
    )


def normalize(tensor, gain):
    widened_values = tensor.astype(F32)
    return (
        widened_values
        * lax.rsqrt(jnp.mean(widened_values * widened_values, axis=-1, keepdims=True) + EPS)
        * gain
    ).astype(BF16)


def shards(
    queries,
    forget_forward_logits,
    forget_backward_logits,
    values,
    output_gate_logits,
    lower_bound_forward,
    lower_bound_backward,
    extra_log_decay,
    head_norm_scale,
    output_projection,
    second_residual,
    expert_norm_scale,
    routes,
    specialist_mixing_factor,
    expert_gate_matrix,
    expert_up_matrix,
    expert_down_matrix,
):
    group_rows, width_model = second_residual.shape
    quarters = lax.axis_size("tp")
    experts = lax.axis_size("ep")
    row_count = group_rows // quarters
    slot_count = 2 * TOPK * row_count // experts
    quarter = lax.axis_index("tp")
    gate_all = lax.all_gather(expert_gate_matrix[0], "tp", axis=0)
    up_all = lax.all_gather(expert_up_matrix[0], "tp", axis=0)
    down_all = lax.all_gather(expert_down_matrix[0], "tp", axis=0, tiled=True)
    own_rows = normalize(
        lax.dynamic_slice_in_dim(second_residual, quarter * row_count, row_count, 0),
        expert_norm_scale,
    )
    flat_routes = lax.dynamic_slice_in_dim(routes, quarter * row_count, row_count, 0).reshape(-1)
    expert_hits = (flat_routes[:, None] == jnp.arange(experts, dtype=jnp.int32)[None, :]).astype(
        jnp.int32
    )
    ranking = jnp.sum(jnp.cumsum(expert_hits, axis=0) * expert_hits, axis=1) - 1
    target = flat_routes * slot_count + ranking
    own_pick = (
        target[:, None] == jnp.arange(experts * slot_count, dtype=jnp.int32)[None, :]
    ).astype(BF16)
    chooser = own_pick.reshape(row_count, TOPK, -1).sum(axis=1)
    outgoing = jnp.einsum("rs,rd->sd", chooser, own_rows, preferred_element_type=F32).astype(BF16)
    mixer_hidden, arrived = mixer(
        experts,
        queries,
        forget_forward_logits,
        forget_backward_logits,
        values,
        output_gate_logits,
        lower_bound_forward,
        lower_bound_backward,
        extra_log_decay,
        head_norm_scale,
        outgoing.reshape(experts, slot_count, width_model),
    )
    mixer_output = lax.psum_scatter(
        jnp.dot(mixer_hidden, output_projection, preferred_element_type=F32).astype(BF16),
        "tp",
        scatter_dimension=0,
        tiled=True,
    )
    rows_in = arrived.reshape(-1, width_model)
    hidden = []
    for part in range(quarters):
        gated = jnp.dot(rows_in, gate_all[part], preferred_element_type=F32)
        lifted = jnp.dot(rows_in, up_all[part], preferred_element_type=F32)
        hidden.append((jax.nn.silu(gated) * lifted).astype(BF16))
    results = jnp.dot(
        jnp.concatenate(hidden, axis=1), down_all, preferred_element_type=F32
    ).astype(BF16)
    returned = exchange(results.reshape(experts, slot_count, width_model), experts)
    gathered = jnp.dot(
        own_pick, returned.reshape(-1, width_model), preferred_element_type=F32
    )
    blended = jnp.sum(
        gathered.reshape(row_count, TOPK, width_model) * specialist_mixing_factor[:, :, None],
        axis=1,
    )
    return (mixer_output, blended.astype(BF16))


def solution(mesh):
    in_specs = (
        P("ep", "tp"),
        P("ep", "tp"),
        P("ep", "tp"),
        P("ep", "tp"),
        P("ep", "tp"),
        P("tp"),
        P("tp"),
        P("ep", "tp"),
        P("tp"),
        P("tp", None),
        P("ep", None),
        P(),
        P("ep", None),
        P(("ep", "tp"), None),
        P("ep", None, "tp"),
        P("ep", None, "tp"),
        P("ep", "tp", None),
    )
    out_specs = (P(("ep", "tp"), None), P(("ep", "tp"), None))
    return jax.shard_map(shards, mesh=mesh, in_specs=in_specs, out_specs=out_specs, check_vma=False)
```

time: 406 us -> 187 us (0.46)
  the two profiles are of different devices: /device:TPU:0 before, /device:TPU:11 now
where the time goes in v1:
time: 187 us; the launch traced here: 186 us
  Pallas kernels  117 us (63%)
  matrix products  29.1 us (16%)
  waiting for transfers between devices  20.8 us (11%)
  between operations  14.1 us (8%)
  local copies, waits for them, and re-layouts  3.52 us (2%)
  other arithmetic  2.08 us (1%)
    pallas_call x1, Pallas kernels, mixer(): pl.pallas_call(functools.partial(mixer_kernel, n), out_shape=(jax.ShapeDt...  64 us
    pallas_call x1, Pallas kernels, exchange(): pl.pallas_call(functools.partial(exchange_kernel, n), out_shape=jax.Shape...  52.6 us
    all_gather x1, waiting for transfers between devices, shards(): down_all = lax.all_gather(expert_down_matrix[0], 'tp', axis=0, tiled=True)  18.7 us
    dot_general x4, matrix products, shards(): gated = jnp.dot(rows_in, gate_all[part], preferred_element_type=F32)  8.91 us
    dot_general x4, matrix products, shards(): lifted = jnp.dot(rows_in, up_all[part], preferred_element_type=F32)  6.86 us
    dot_general x1, matrix products, shards(): jnp.dot(jnp.concatenate(hidden, axis=1), down_all, preferred_element_type...  6.13 us
  transfers between devices with their start and end apart: 4, of which 1 were waited for; matrix products, arithmetic and copies ran while one was open for 17% of the time, Pallas kernels for 63%

profile of v1, /device:TPU:11, one launch (start us, length us, event | category | flops | bytes accessed | tf_op | source)
XLA Modules:
  0.0 186.3 jit_solution(16508394122019491919)
XLA Ops:
  7.2 0.0 copy-start
  7.2 0.0 copy-start.13
  7.2 0.0 copy-start.12
  7.2 0.0 copy-start.11
  7.2 0.0 all-gather.5.cloned.1.call-start
  7.3 0.7 all-gather.5.cloned.1.call-update
  7.9 0.0 all-gather.7.cloned.1.call-start
  8.0 0.7 all-gather.7.cloned.1.call-update
  8.7 0.0 all-gather.9.cloned.1.call-start
  8.7 0.7 all-gather.9.cloned.1.call-update
  9.4 0.0 copy-start.1
  9.4 0.0 copy-start.2
  9.5 0.0 copy-start.3
  9.5 0.0 reduce-scatter.2.cloned.1.call-start
  9.6 0.1 copy.31
  9.7 0.1 eq.65
  9.8 0.1 eq.61
  10.0 0.6 reduce-window.6
  10.6 0.2 slice_reduce_fusion
  10.8 0.1 fusion.33
  10.9 0.1 sub.7
  11.1 0.1 copy.33
  11.2 0.2 copy.34.extra_ref
  11.3 1.2 fusion.10
  12.6 0.1 fusion.31
  12.7 0.0 copy-done.11
  12.7 1.8 convolution_convert_fusion.1
  14.7 64.0 %mix_dispatch.1 = (bf16[512,256]{1,0:T(8,128)(2,1)S(1)}, bf16[8,64,2048]{2,1,0:T(8,128)(2,1)S(1)}) custom-call(bf16[512,256]{1,0:T(8,128)(2,1)S(1)} %copy-done.1, bf16[512,256]{1,0:T(8,128)(2,1)S(1)} %copy-done.2, bf16[512,256]{1,0:T(8,128)(2,1)S(1)} %copy-done.3, bf16[512,256]{1,0:T(8,128)(2,1)S(1)} %copy-done.4, bf16[512,256]{1,0:T(8,128)(2,1)S(1)} %copy-done.5, ...), custom_call_target="tpu_custom_call" | custom-call | flops 40000000000 | bytes 6291456 | tf_op jit(solution)/shard_map/mix_dispatch/pallas_call | solution.py:267
  78.7 1.3 copy-done.9
  80.0 0.0 copy-done
  80.0 2.0 %convolution_convert_fusion = bf16[512,2048]{1,0:T(8,128)(2,1)} fusion(bf16[512,256]{1,0:T(8,128)(2,1)S(1)} %get-tuple-element.4, bf16[256,2048]{1,0:T(8,128)(2,1)S(1)} %copy-done), kind=kOutput, calls=%fused_computation.3 | convolution fusion | flops 537919488 | bytes 3407872 | tf_op jit(solution)/shard_map/dot_general | solution.py:374
  82.0 0.0 reduce-scatter.2.cloned.1.call-update
  82.1 0.0 all-gather.5.cloned.1.call-done
  82.1 2.9 %fusion.16 = f32[512,256]{0,1:T(8,128)} fusion(bf16[512,2048]{1,0:T(8,128)(2,1)S(1)} %bitcast.63, bf16[4,2048,256]{2,1,0:T(8,128)(2,1)} %all-gather.5.cloned.1.call-done), kind=kOutput, calls=%fused_computation.31 | convolution fusion | flops 536870912 | bytes 3670016 | tf_op jit(solution)/shard_map/dot_general | solution.py:382
  85.0 2.8 %fusion.15 = f32[512,256]{0,1:T(8,128)} fusion(bf16[512,2048]{1,0:T(8,128)(2,1)S(1)} %bitcast.64, bf16[4,2048,256]{2,1,0:T(8,128)(2,1)} %all-gather.5.cloned.1.call-done), kind=kOutput, calls=%fused_computation.28 | convolution fusion | flops 536870912 | bytes 3670016 | tf_op jit(solution)/shard_map/dot_general | solution.py:382
  87.8 1.6 fusion.14
  89.4 1.6 fusion.13
  91.0 2.4 %fusion.6 = bf16[512,256]{0,1:T(8,128)(2,1)S(1)} fusion(bf16[512,2048]{1,0:T(8,128)(2,1)S(1)} %bitcast.67, bf16[4,2048,256]{2,1,0:T(8,128)(2,1)} %all-gather.7.cloned.1.call-done, f32[512,256]{0,1:T(8,128)} %fusion.16), kind=kOutput, calls=%fused_computation.13 | convolution fusion | flops 537657344 | bytes 3932160 | tf_op jit(solution)/shard_map/dot_general | solution.py:383
  93.4 1.0 copy-done.14
  94.4 0.1 copy-done.19
  94.6 1.5 fusion.7
  96.1 1.5 fusion.8
  97.6 1.5 fusion.9
  99.1 18.7 %all-gather.9.cloned.1.call-done = bf16[1,1024,2048]{2,1,0:T(8,128)(2,1)} async-done(((bf16[1,256,2048]{2,1,0:T(8,128)(2,1)}), bf16[1,1024,2048]{2,1,0:T(8,128)(2,1)}) %all-gather.9.cloned.1.call-update) | async-done | bytes 4194320 | tf_op jit(solution)/shard_map/all_gather | solution.py:344
  117.7 6.1 %fusion.2 = bf16[512,2048]{1,0:T(8,128)(2,1)} fusion(bf16[1,1024,2048]{2,1,0:T(8,128)(2,1)} %all-gather.9.cloned.1.call-done, bf16[512,256]{0,1:T(8,128)(2,1)} %fusion.9, bf16[512,256]{0,1:T(8,128)(2,1)} %fusion.8, bf16[512,256]{0,1:T(8,128)(2,1)} %fusion.7, bf16[512,256]{0,1:T(8,128)(2,1)S(1)} %fusion.6), kind=kOutput, calls=%fused_computation.2 | convolution fusion | flops 2152726528 | bytes 7340032 | tf_op jit(solution)/shard_map/dot_general | solution.py:385
  123.9 52.6 %return_rows.1 = bf16[8,64,2048]{2,1,0:T(8,128)(2,1)} custom-call(bf16[8,64,2048]{2,1,0:T(8,128)(2,1)} %bitcast.71), custom_call_target="tpu_custom_call" | custom-call | flops 20000000000 | bytes 4194304 | tf_op jit(solution)/shard_map/return_rows/pallas_call | solution.py:78
  176.4 0.0 copy-done.16
  176.4 3.3 %fusion.5 = bf16[128,2048]{1,0:T(8,128)(2,1)} fusion(bf16[512,2048,1]{1,0,2:T(8,128)(2,1)} %bitcast.72, f32[128,2]{0,1:T(2,128)S(1)} %copy-done.16, s32[128,2]{0,1:T(2,128)S(1)} %multiply_add_fusion), kind=kOutput, calls=%fused_computation.6 | convolution fusion | flops 537788416 | bytes 2623488 | tf_op jit(solution)/shard_map/dot_general | solution.py:389
  (36 shorter events, 0.1 us)
Async XLA Ops:
  7.2 72.8 %copy-start = (bf16[256,2048]{1,0:T(8,128)(2,1)S(1)}, bf16[256,2048]{1,0:T(8,128)(2,1)}, u32[]{:S(2)}) copy-start(bf16[256,2048]{1,0:T(8,128)(2,1)} %param.26) | copy-start | bytes 3145732
  7.2 2.4 %copy-start.13 = (s32[512,2]{0,1:T(2,128)S(1)}, s32[512,2]{0,1:T(2,128)}, u32[]{:S(2)}) copy-start(s32[512,2]{0,1:T(2,128)} %param.29) | copy-start | bytes 12292
  7.2 4.0 %copy-start.12 = (f32[512,2]{0,1:T(2,128)S(1)}, f32[512,2]{0,1:T(2,128)}, u32[]{:S(2)}) copy-start(f32[512,2]{0,1:T(2,128)} %param.24) | copy-start | bytes 12292
  7.2 5.5 %copy-start.11 = (f32[2048]{0:T(1024)S(1)}, f32[2048]{0:T(1024)}, u32[]{:S(2)}) copy-start(f32[2048]{0:T(1024)} %param.28) | copy-start | bytes 24580
  7.2 74.9 %all-gather.5.cloned.1.call-start = ((), (), s32[]{:S(2)}) async-start(), calls=%async_computation.2 | async-start | bytes 5242880 | tf_op jit(solution)/shard_map/all_gather | solution.py:342
  7.9 83.1 %all-gather.7.cloned.1.call-start = ((), (), s32[]{:S(2)}) async-start(), calls=%async_computation.3 | async-start | bytes 5242880 | tf_op jit(solution)/shard_map/all_gather | solution.py:343
  8.7 109.0 %all-gather.9.cloned.1.call-start = ((), (), s32[]{:S(2)}) async-start(), calls=%async_computation.4 | async-start | bytes 5242880 | tf_op jit(solution)/shard_map/all_gather | solution.py:344
  9.4 5.1 %copy-start.1 = (bf16[512,256]{1,0:T(8,128)(2,1)S(1)}, bf16[512,256]{1,0:T(8,128)(2,1)}, u32[]{:S(2)}) copy-start(bf16[512,256]{1,0:T(8,128)(2,1)} %q_ref.1) | copy-start | bytes 786436
  9.4 5.1 %copy-start.2 = (bf16[512,256]{1,0:T(8,128)(2,1)S(1)}, bf16[512,256]{1,0:T(8,128)(2,1)}, u32[]{:S(2)}) copy-start(bf16[512,256]{1,0:T(8,128)(2,1)} %ff_ref.1) | copy-start | bytes 786436
  9.5 5.1 %copy-start.3 = (bf16[512,256]{1,0:T(8,128)(2,1)S(1)}, bf16[512,256]{1,0:T(8,128)(2,1)}, u32[]{:S(2)}) copy-start(bf16[512,256]{1,0:T(8,128)(2,1)} %fb_ref.1) | copy-start | bytes 786436
  9.5 5.1 %copy-start.4 = (bf16[512,256]{1,0:T(8,128)(2,1)S(1)}, bf16[512,256]{1,0:T(8,128)(2,1)}, u32[]{:S(2)}) copy-start(bf16[512,256]{1,0:T(8,128)(2,1)} %v_ref.1) | copy-start | bytes 786436
  9.5 5.1 %copy-start.5 = (bf16[512,256]{1,0:T(8,128)(2,1)S(1)}, bf16[512,256]{1,0:T(8,128)(2,1)}, u32[]{:S(2)}) copy-start(bf16[512,256]{1,0:T(8,128)(2,1)} %og_ref.1) | copy-start | bytes 786436
  9.5 5.1 %copy-start.6 = (f32[256]{0:T(256)S(1)}, f32[256]{0:T(256)}, u32[]{:S(2)}) copy-start(f32[256]{0:T(256)} %param.22) | copy-start | bytes 3076
  9.5 5.1 %copy-start.7 = (f32[256]{0:T(256)S(1)}, f32[256]{0:T(256)}, u32[]{:S(2)}) copy-start(f32[256]{0:T(256)} %param.23) | copy-start | bytes 3076
  9.5 5.1 %copy-start.8 = (f32[256]{0:T(256)S(1)}, f32[256]{0:T(256)}, u32[]{:S(2)}) copy-start(f32[256]{0:T(256)} %param.25) | copy-start | bytes 3076
  9.5 170.3 %reduce-scatter.2.cloned.1.call-start = ((), (), s32[]{:S(2)}) async-start(), calls=%async_computation.1 | async-start | bytes 2621440 | tf_op jit(solution)/shard_map/reduce_scatter | solution.py:373
  78.7 1.3 copy-start.9
  80.0 2.1 %copy-start.10 = (bf16[8,64,2048]{2,1,0:T(8,128)(2,1)S(1)}, bf16[8,64,2048]{2,1,0:T(8,128)(2,1)}, u32[]{:S(2)}) copy-start(bf16[8,64,2048]{2,1,0:T(8,128)(2,1)} %copy-done.9) | copy-start | bytes 6291460
  82.1 5.7 %copy-start.15 = (bf16[4,2048,256]{2,1,0:T(8,128)(2,1)S(1)}, bf16[4,2048,256]{2,1,0:T(8,128)(2,1)}, u32[]{:S(2)}) copy-start(bf16[4,2048,256]{2,1,0:T(8,128)(2,1)} %all-gather.5.cloned.1.call-done) | copy-start | bytes 12582916
  91.0 3.4 %copy-start.14 = (bf16[4,2048,256]{2,1,0:T(8,128)(2,1)S(1)}, bf16[4,2048,256]{2,1,0:T(8,128)(2,1)}, u32[]{:S(2)}) copy-start(bf16[4,2048,256]{2,1,0:T(8,128)(2,1)} %all-gather.7.cloned.1.call-done) | copy-start | bytes 12582916
  91.0 3.5 %copy-start.19 = (f32[512,256]{0,1:T(8,128)S(1)}, f32[512,256]{0,1:T(8,128)}, u32[]{:S(2)}) copy-start(f32[512,256]{0,1:T(8,128)} %fusion.15) | copy-start | bytes 1572868
  94.6 1.5 copy-start.18
  96.1 1.5 copy-start.17
  123.9 52.6 %copy-start.16 = (f32[128,2]{0,1:T(2,128)S(1)}, f32[128,2]{0,1:T(2,128)}, u32[]{:S(2)}) copy-start(f32[128,2]{0,1:T(2,128)} %param.30) | copy-start | bytes 3076
Sparse Core Ops, SparseCore 0:
  9.6 35.9 all-gather.4
  47.2 34.4 all-gather.6
  83.2 34.4 all-gather.8
  120.7 30.5 reduce-scatter.1

commit v2 on v1

--- a/solution.py
+++ b/solution.py
@@ -17,49 +17,52 @@
 BF16 = jnp.bfloat16
 
 
-def greet(n):
-    me = lax.axis_index("ep")
+def neighbours():
+    place, count = lax.axis_index("tp"), lax.axis_size("tp")
+    return place + 1 - 2 * lax.rem(place, 2), lax.rem(place + count // 2, count)
+
+
+def greet(axis, n):
+    me = lax.axis_index(axis)
     barrier = pltpu.get_barrier_semaphore()
 
     def one(step, carry):
         peer = lax.rem(me + step, n)
-        pl.semaphore_signal(barrier, inc=1, device_id={"ep": peer}, device_id_type=MESH)
+        pl.semaphore_signal(barrier, inc=1, device_id={axis: peer}, device_id_type=MESH)
         return carry
 
     lax.fori_loop(1, n, one, 0)
-    pl.semaphore_wait(barrier, n - 1)
-
-
-def block_copy(out_ref, in_ref, send_sem, recv_sem, target, source):
-    me = lax.axis_index("ep")
+
+
+def block_copy(axis, out_ref, in_ref, send_sem, recv_sem, target, source):
     return pltpu.make_async_remote_copy(
         src_ref=out_ref.at[target],
         dst_ref=in_ref.at[source],
         send_sem=send_sem.at[target],
         recv_sem=recv_sem.at[source],
-        device_id={"ep": target},
+        device_id={axis: target},
         device_id_type=MESH,
     )
 
 
-def start_blocks(n, out_ref, in_ref, send_sem, recv_sem):
-    me = lax.axis_index("ep")
+def start_blocks(axis, n, out_ref, in_ref, send_sem, recv_sem):
+    me = lax.axis_index(axis)
 
     def one(step, carry):
         peer = lax.rem(me + step, n)
-        block_copy(out_ref, in_ref, send_sem, recv_sem, peer, me).start()
+        block_copy(axis, out_ref, in_ref, send_sem, recv_sem, peer, me).start()
         return carry
 
     lax.fori_loop(1, n, one, 0)
     in_ref[me] = out_ref[me]
 
 
-def finish_blocks(n, out_ref, in_ref, send_sem, recv_sem):
-    me = lax.axis_index("ep")
+def finish_blocks(axis, n, out_ref, in_ref, send_sem, recv_sem):
+    me = lax.axis_index(axis)
 
     def one(step, carry):
         peer = lax.rem(me + step, n)
-        copy = block_copy(out_ref, in_ref, send_sem, recv_sem, peer, peer)
+        copy = block_copy(axis, out_ref, in_ref, send_sem, recv_sem, peer, peer)
         copy.wait_send()
         copy.wait_recv()
         return carry
@@ -67,26 +70,40 @@
     lax.fori_loop(1, n, one, 0)
 
 
-def exchange_kernel(n, out_ref, in_ref, send_sem, recv_sem):
-    greet(n)
-    start_blocks(n, out_ref, in_ref, send_sem, recv_sem)
-    finish_blocks(n, out_ref, in_ref, send_sem, recv_sem)
-
-
-def exchange(blocks, n):
+def exchange_kernel(n, quarters, rows_ref, part_ref, back_ref, sums_ref, *sems):
+    greet("ep", n)
+    greet("tp", quarters)
+    pl.semaphore_wait(pltpu.get_barrier_semaphore(), n + quarters - 2)
+    start_blocks("ep", n, rows_ref, back_ref, *sems[:2])
+    start_blocks("tp", quarters, part_ref, sums_ref, *sems[2:])
+    finish_blocks("tp", quarters, part_ref, sums_ref, *sems[2:])
+    finish_blocks("ep", n, rows_ref, back_ref, *sems[:2])
+
+
+def exchange(blocks, partials, n, quarters):
     vmem = pl.BlockSpec(memory_space=pltpu.VMEM)
     return pl.pallas_call(
-        functools.partial(exchange_kernel, n),
-        out_shape=jax.ShapeDtypeStruct(blocks.shape, blocks.dtype),
-        in_specs=[vmem],
-        out_specs=vmem,
-        scratch_shapes=[pltpu.SemaphoreType.DMA((n,)), pltpu.SemaphoreType.DMA((n,))],
-        compiler_params=pltpu.CompilerParams(collective_id=1, has_side_effects=True),
+        functools.partial(exchange_kernel, n, quarters),
+        out_shape=(
+            jax.ShapeDtypeStruct(blocks.shape, blocks.dtype),
+            jax.ShapeDtypeStruct(partials.shape, partials.dtype),
+        ),
+        in_specs=[vmem, vmem],
+        out_specs=(vmem, vmem),
+        scratch_shapes=[
+            pltpu.SemaphoreType.DMA((n,)),
+            pltpu.SemaphoreType.DMA((n,)),
+            pltpu.SemaphoreType.DMA((quarters,)),
+            pltpu.SemaphoreType.DMA((quarters,)),
+        ],
+        compiler_params=pltpu.CompilerParams(
+            collective_id=1, has_side_effects=True, vmem_limit_bytes=32 * 2**20
+        ),
         cost_estimate=pl.CostEstimate(
-            flops=2 * 10**10, bytes_accessed=2 * blocks.size * 2, transcendentals=0
+            flops=2 * 10**10, bytes_accessed=4 * blocks.size * 2, transcendentals=0
         ),
         name="return_rows",
-    )(blocks)
+    )(blocks, partials)
 
 
 def dot_rows(a, b):
@@ -139,8 +156,14 @@
     extra_ref,
     scale_ref,
     slots_ref,
+    gate_ref,
+    up_ref,
+    down_ref,
     hidden_ref,
     arrived_ref,
+    gates_ref,
+    ups_ref,
+    downs_ref,
     local_ref,
     reach_ref,
     part_ref,
@@ -151,14 +174,38 @@
     slot_recv,
     state_send,
     state_recv,
+    weight_send,
+    weight_recv,
 ):
     me = lax.axis_index("ep")
     row_count, width = q_ref.shape
     chunks = row_count // CHUNK
     heads = extra_ref.shape[1]
     channels = width // heads
-    greet(n)
-    start_blocks(n, slots_ref, arrived_ref, slot_send, slot_recv)
+    beside, across = neighbours()
+    greet("ep", n)
+    barrier = pltpu.get_barrier_semaphore()
+    for peer in (beside, across):
+        pl.semaphore_signal(barrier, inc=1, device_id={"tp": peer}, device_id_type=MESH)
+    pl.semaphore_wait(barrier, n + 1)
+    weights = ((gate_ref, gates_ref), (up_ref, ups_ref), (down_ref, downs_ref))
+
+    def weight_copy(i, hop):
+        own, held = weights[i]
+        return pltpu.make_async_remote_copy(
+            src_ref=held.at[1] if hop == 2 else own,
+            dst_ref=held.at[hop],
+            send_sem=weight_send.at[i, hop],
+            recv_sem=weight_recv.at[i, hop],
+            device_id={"tp": across if hop == 1 else beside},
+            device_id_type=MESH,
+        )
+
+    for i in range(3):
+        weight_copy(i, 1).start()
+    start_blocks("ep", n, slots_ref, arrived_ref, slot_send, slot_recv)
+    for i in range(3):
+        weight_copy(i, 0).start()
     rows = lax.broadcasted_iota(jnp.int32, (CHUNK, CHUNK), 0)
     cols = lax.broadcasted_iota(jnp.int32, (CHUNK, CHUNK), 1)
 
@@ -230,6 +277,8 @@
         return carry
 
     lax.fori_loop(1, n, send, 0)
+    weight_copy(0, 1).wait_recv()
+    weight_copy(0, 2).start()
     lax.fori_loop(1, n, receive, 0)
     depth = part_ref.shape[3]
     for h in range(heads):
@@ -253,25 +302,35 @@
             gate = og_ref[at, lanes].astype(F32)
             opened = combined * lax.rsqrt(mean_square + EPS) * scale_ref[:, lanes]
             hidden_ref[at, lanes] = (opened * (gate / (1.0 + jnp.exp(-gate)))).astype(BF16)
-    finish_blocks(n, slots_ref, arrived_ref, slot_send, slot_recv)
-
-
-def mixer(n, queries, ff, fb, values, og, lbf, lbb, extra, scale, slots):
+    for i in (1, 2):
+        weight_copy(i, 1).wait_recv()
+        weight_copy(i, 2).start()
+    finish_blocks("ep", n, slots_ref, arrived_ref, slot_send, slot_recv)
+    for i in range(3):
+        weight_copy(i, 1).wait_send()
+        for hop in (0, 2):
+            weight_copy(i, hop).wait_send()
+            weight_copy(i, hop).wait_recv()
+
+
+def mixer(n, queries, ff, fb, values, og, lbf, lbb, extra, scale, slots, gate, up, down):
     row_count, width = queries.shape
     heads = extra.shape[1]
     channels = width // heads
     depth = values.shape[1] // heads
     chunks = row_count // CHUNK
     vmem = pl.BlockSpec(memory_space=pltpu.VMEM)
+    anywhere = pl.BlockSpec(memory_space=pl.ANY)
     state = (heads, depth + DECAY_ROWS, channels)
     return pl.pallas_call(
         functools.partial(mixer_kernel, n),
         out_shape=(
             jax.ShapeDtypeStruct(values.shape, BF16),
             jax.ShapeDtypeStruct(slots.shape, slots.dtype),
-        ),
-        in_specs=[vmem] * 10,
-        out_specs=(vmem, vmem),
+        )
+        + tuple(jax.ShapeDtypeStruct((3,) + w.shape, w.dtype) for w in (gate, up, down)),
+        in_specs=[vmem] * 10 + [anywhere] * 3,
+        out_specs=(vmem, vmem) + (anywhere,) * 3,
         scratch_shapes=[
             pltpu.VMEM((heads, chunks, CHUNK, depth), F32),
             pltpu.VMEM((2, heads, chunks, CHUNK, channels), BF16),
@@ -283,6 +342,8 @@
             pltpu.SemaphoreType.DMA((n,)),
             pltpu.SemaphoreType.DMA((n,)),
             pltpu.SemaphoreType.DMA((n,)),
+            pltpu.SemaphoreType.DMA((3, 3)),
+            pltpu.SemaphoreType.DMA((3, 3)),
         ],
         compiler_params=pltpu.CompilerParams(
             collective_id=0, has_side_effects=True, vmem_limit_bytes=48 * 2**20
@@ -302,6 +363,9 @@
         extra,
         scale.reshape(1, -1),
         slots,
+        gate,
+        up,
+        down,
     )
 
 
@@ -339,9 +403,7 @@
     row_count = group_rows // quarters
     slot_count = 2 * TOPK * row_count // experts
     quarter = lax.axis_index("tp")
-    gate_all = lax.all_gather(expert_gate_matrix[0], "tp", axis=0)
-    up_all = lax.all_gather(expert_up_matrix[0], "tp", axis=0)
-    down_all = lax.all_gather(expert_down_matrix[0], "tp", axis=0, tiled=True)
+    gate, up, down = expert_gate_matrix[0], expert_up_matrix[0], expert_down_matrix[0]
     own_rows = normalize(
         lax.dynamic_slice_in_dim(second_residual, quarter * row_count, row_count, 0),
         expert_norm_scale,
@@ -357,7 +419,7 @@
     ).astype(BF16)
     chooser = own_pick.reshape(row_count, TOPK, -1).sum(axis=1)
     outgoing = jnp.einsum("rs,rd->sd", chooser, own_rows, preferred_element_type=F32).astype(BF16)
-    mixer_hidden, arrived = mixer(
+    mixer_hidden, arrived, gates_held, ups_held, downs_held = mixer(
         experts,
         queries,
         forget_forward_logits,
@@ -369,23 +431,30 @@
         extra_log_decay,
         head_norm_scale,
         outgoing.reshape(experts, slot_count, width_model),
-    )
-    mixer_output = lax.psum_scatter(
-        jnp.dot(mixer_hidden, output_projection, preferred_element_type=F32).astype(BF16),
-        "tp",
-        scatter_dimension=0,
-        tiled=True,
-    )
+        gate,
+        up,
+        down,
+    )
+    partials = jnp.dot(mixer_hidden, output_projection, preferred_element_type=F32).astype(BF16)
     rows_in = arrived.reshape(-1, width_model)
-    hidden = []
-    for part in range(quarters):
-        gated = jnp.dot(rows_in, gate_all[part], preferred_element_type=F32)
-        lifted = jnp.dot(rows_in, up_all[part], preferred_element_type=F32)
-        hidden.append((jax.nn.silu(gated) * lifted).astype(BF16))
-    results = jnp.dot(
-        jnp.concatenate(hidden, axis=1), down_all, preferred_element_type=F32
-    ).astype(BF16)
-    returned = exchange(results.reshape(experts, slot_count, width_model), experts)
+
+    def hidden_part(gate_part, up_part):
+        gated = jnp.dot(rows_in, gate_part, preferred_element_type=F32)
+        lifted = jnp.dot(rows_in, up_part, preferred_element_type=F32)
+        return (jax.nn.silu(gated) * lifted).astype(BF16)
+
+    result = jnp.dot(hidden_part(gate, up), down, preferred_element_type=F32)
+    rest = jnp.concatenate([hidden_part(gates_held[i], ups_held[i]) for i in range(3)], axis=1)
+    result = result + jnp.dot(
+        rest, downs_held.reshape(-1, width_model), preferred_element_type=F32
+    )
+    returned, pieces = exchange(
+        result.astype(BF16).reshape(experts, slot_count, width_model),
+        partials.reshape(quarters, row_count, width_model),
+        experts,
+        quarters,
+    )
+    mixer_output = jnp.sum(pieces.astype(F32), axis=0).astype(BF16)
     gathered = jnp.dot(
         own_pick, returned.reshape(-1, width_model), preferred_element_type=F32
     )

time: 187 us -> 170 us (0.909)
  waiting for transfers between devices: 20.8 us -> 0 us
  between operations: 14.1 us -> 0.95 us
  Pallas kernels: 117 us -> 128 us
  local copies, waits for them, and re-layouts: 3.52 us -> 9.6 us
  matrix products: 29.1 us -> 25.7 us
  other arithmetic: 2.08 us -> 4.76 us
    all_gather x3 -> x0, waiting for transfers between devices: 18.7 us -> none  [the longest x1 18.7 us: shards(): down_all = lax.all_gather(expert_down_matrix[0], 'tp', axis=0, tiled=True)]
    pallas_call x1, Pallas kernels: 64 us -> 78.5 us  [mixer(): pl.pallas_call(functools.partial(mixer_kernel, n), out_shape=(jax.ShapeDt...]
    unnamed x41 -> x43, local copies, waits for them, and re-layouts: 2.7 us -> 8.11 us
    dot_general x9, matrix products: 21.9 us -> 18.3 us  [the longest x1 6.67 us: shards(): result = jnp.dot(hidden_part(gate, up), down, preferred_element_type=F32)]
    pallas_call x1, Pallas kernels: 52.6 us -> 49.2 us  [exchange(): pl.pallas_call(functools.partial(exchange_kernel, n, quarters), out_shape...]
    unnamed x4 -> x0, waiting for transfers between devices: 2.07 us -> none
  transfers between devices with their start and end apart: 4 -> 0, of which waited for: 1 -> 0; matrix products, arithmetic and copies ran while one was open for 17% -> 0% of each run, Pallas kernels for 63% -> 0%
where the time goes in v2:
time: 170 us; the launch traced here: 169 us
  Pallas kernels  128 us (75%)
  matrix products  25.7 us (15%)
  local copies, waits for them, and re-layouts  9.6 us (6%)
  other arithmetic  4.76 us (3%)
    pallas_call x1, Pallas kernels, mixer(): pl.pallas_call(functools.partial(mixer_kernel, n), out_shape=(jax.ShapeDt...  78.5 us
    pallas_call x1, Pallas kernels, exchange(): pl.pallas_call(functools.partial(exchange_kernel, n, quarters), out_shape...  49.2 us
    unnamed x43, local copies, waits for them, and re-layouts  8.11 us
    dot_general x1, matrix products, shards(): result = jnp.dot(hidden_part(gate, up), down, preferred_element_type=F32)  6.67 us
    dot_general x4, matrix products, hidden_part(): gated = jnp.dot(rows_in, gate_part, preferred_element_type=F32)  5.7 us
    dot_general x1, matrix products, shards(): jnp.dot(rest, downs_held.reshape(-1, width_model), preferred_element_type...  3.72 us
    dot_general x1, matrix products, shards(): jnp.einsum('rs,rd->sd', chooser, own_rows, preferred_element_type=F32)  3.43 us

profile of v2, /device:TPU:11, one launch (start us, length us, event | category | flops | bytes accessed | tf_op | source)
XLA Modules:
  0.0 168.8 jit_solution(4752923347657719068)
XLA Ops:
  0.6 0.0 copy-start
  0.6 0.0 copy-start.3
  0.7 0.0 copy-start.2
  0.7 0.0 copy-start.14
  0.7 1.4 fusion.5
  2.1 0.5 add_rsqrt_fusion
  2.6 0.7 constant_dynamic-slice_fusion
  3.3 0.1 copy.49
  3.4 0.1 eq.65
  3.5 0.1 eq.61
  3.7 0.6 reduce-window.6
  4.3 0.2 slice_reduce_fusion
  4.5 0.1 fusion.44
  4.6 0.1 sub.7
  4.8 0.1 copy.51
  4.9 0.7 multiply_add_fusion
  5.6 0.1 fusion.41
  5.7 0.8 copy.52.extra_ref
  6.5 0.0 copy-start.6
  6.5 0.0 copy-start.7
  6.5 0.0 copy-start.8
  6.6 0.0 copy-start.9
  6.6 3.4 %convolution_convert_fusion.1 = bf16[512,2048]{1,0:T(8,128)(2,1)} fusion(bf16[128,512]{1,0:T(8,128)(2,1)S(1)} %fusion.41, f32[2048]{0:T(1024)} %param.28, f32[128]{0:T(128)} %add_rsqrt_fusion, bf16[512,2048]{1,0:T(8,128)(2,1)} %param.27, s32[]{:T(128)S(6)} %select_n.4), kind=kOutput, calls=%fused_computation.2 | convolution fusion | flops 270532608 | bytes 2761220 | tf_op jit(solution)/shard_map/rs,rd->sd/dot_general | solution.py:421
  10.0 0.0 copy-done.3
  10.1 0.0 copy-start.10
  10.1 0.9 copy-done.10
  11.0 0.9 copy-done.11
  12.0 78.5 %mix_dispatch.1 = (bf16[512,256]{1,0:T(8,128)(2,1)S(1)}, bf16[8,64,2048]{2,1,0:T(8,128)(2,1)}, bf16[3,2048,256]{2,1,0:T(8,128)(2,1)}, bf16[3,2048,256]{2,1,0:T(8,128)(2,1)}, bf16[3,256,2048]{2,1,0:T(8,128)(2,1)}) custom-call(bf16[512,256]{1,0:T(8,128)(2,1)S(1)} %copy-done.7, bf16[512,256]{1,0:T(8,128)(2,1)S(1)} %copy-done.8, bf16[512,256]{1,0:T(8,128)(2,1)S(1)} %copy-done.9, ...), custom_call_target="tpu_custom_call" | custom-call | flops 40000000000 | bytes 6291456 | tf_op jit(solution)/shard_map/mix_dispatch/pallas_call | solution.py:325
  90.5 0.0 copy-start.4
  90.6 2.7 %fusion.9 = f32[512,256]{1,0:T(8,128)S(1)} fusion(bf16[512,2048]{1,0:T(8,128)(2,1)} %bitcast.71, bf16[3,2048,256]{2,1,0:T(8,128)(2,1)} %get-tuple-element.10), kind=kOutput, calls=%fused_computation.19 | convolution fusion | flops 536870912 | bytes 3670016 | tf_op jit(solution)/shard_map/dot_general | solution.py:442
  93.3 0.8 copy-done.20
  94.1 0.7 fusion.4
  94.8 1.2 copy-done.19
  96.0 0.7 fusion.12
  96.7 0.7 fusion.15
  97.5 0.7 fusion.2
  98.2 0.7 fusion.3
  98.9 1.2 copy-done.18
  100.1 3.7 %fusion.23 = f32[512,2048]{1,0:T(8,128)} fusion(bf16[768,2048]{1,0:T(8,128)(2,1)S(1)} %bitcast.79, bf16[512,256]{1,0:T(8,128)(2,1)S(1)} %fusion.4, bf16[512,256]{1,0:T(8,128)(2,1)S(1)} %fusion.3, bf16[512,256]{1,0:T(8,128)(2,1)S(1)} %fusion.2), kind=kOutput, calls=%fused_computation.33 | convolution fusion | flops 1612972032 | bytes 8126464 | tf_op jit(solution)/shard_map/dot_general | solution.py:448
  103.8 1.5 fusion.51
  105.3 6.7 %add_convert_fusion = bf16[512,2048]{1,0:T(8,128)(2,1)} fusion(f32[512,2048]{1,0:T(8,128)} %fusion.23, bf16[512,2048]{1,0:T(8,128)(2,1)} %bitcast.72, f32[512,256]{1,0:T(8,128)} %fusion.51, bf16[1,256,2048]{2,1,0:T(8,128)(2,1)S(1)} %copy-done.3, bf16[1,2048,256]{2,1,0:T(8,128)(2,1)S(1)} %copy-done.2), kind=kOutput, calls=%fused_computation | convolution fusion | flops 1076625408 | bytes 11010048 | tf_op jit(solution)/shard_map/dot_general | solution.py:446
  112.0 0.7 convolution_convert_fusion
  112.7 0.9 copy-done.1
  113.6 49.2 %return_rows.1 = (bf16[8,64,2048]{2,1,0:T(8,128)(2,1)S(1)}, bf16[4,128,2048]{2,1,0:T(8,128)(2,1)S(1)}) custom-call(bf16[8,64,2048]{2,1,0:T(8,128)(2,1)S(1)} %bitcast.62, bf16[4,128,2048]{2,1,0:T(8,128)(2,1)S(1)} %bitcast.61), custom_call_target="tpu_custom_call" | custom-call | flops 20000000000 | bytes 8388608 | tf_op jit(solution)/shard_map/return_rows/pallas_call | solution.py:85
  162.8 1.3 copy-done.15
  164.1 1.3 reduce_sum.54
  165.4 0.0 copy-done.17
  165.4 3.3 %fusion = bf16[128,2048]{1,0:T(8,128)(2,1)} fusion(bf16[512,2048,1]{1,0,2:T(8,128)(2,1)} %bitcast.69, f32[128,2]{0,1:T(2,128)S(1)} %copy-done.17, s32[128,2]{0,1:T(2,128)S(1)} %multiply_add_fusion), kind=kOutput, calls=%fused_computation.4 | convolution fusion | flops 537788416 | bytes 2623488 | tf_op jit(solution)/shard_map/dot_general | solution.py:458
  (27 shorter events, 0.1 us)
Async XLA Ops:
  0.6 111.4 %copy-start = (bf16[256,2048]{1,0:T(8,128)(2,1)S(1)}, bf16[256,2048]{1,0:T(8,128)(2,1)}, u32[]{:S(2)}) copy-start(bf16[256,2048]{1,0:T(8,128)(2,1)} %param.26) | copy-start | bytes 3145732
  0.6 9.3 %copy-start.3 = (bf16[1,256,2048]{2,1,0:T(8,128)(2,1)S(1)}, bf16[1,256,2048]{2,1,0:T(8,128)(2,1)}, u32[]{:S(2)}) copy-start(bf16[1,256,2048]{2,1,0:T(8,128)(2,1)} %param.33) | copy-start | bytes 3145732
  0.7 9.3 %copy-start.2 = (bf16[1,2048,256]{2,1,0:T(8,128)(2,1)S(1)}, bf16[1,2048,256]{2,1,0:T(8,128)(2,1)}, u32[]{:S(2)}) copy-start(bf16[1,2048,256]{2,1,0:T(8,128)(2,1)} %param.32) | copy-start | bytes 3145732
  0.7 9.3 %copy-start.14 = (f32[256]{0:T(256)S(1)}, f32[256]{0:T(256)}, u32[]{:S(2)}) copy-start(f32[256]{0:T(256)} %param.25) | copy-start | bytes 3076
  0.7 9.3 %copy-start.13 = (f32[256]{0:T(256)S(1)}, f32[256]{0:T(256)}, u32[]{:S(2)}) copy-start(f32[256]{0:T(256)} %param.23) | copy-start | bytes 3076
  0.7 9.3 %copy-start.12 = (f32[256]{0:T(256)S(1)}, f32[256]{0:T(256)}, u32[]{:S(2)}) copy-start(f32[256]{0:T(256)} %param.22) | copy-start | bytes 3076
  6.5 3.5 %copy-start.6 = (bf16[1,2048,256]{2,1,0:T(8,128)(2,1)S(1)}, bf16[1,2048,256]{2,1,0:T(8,128)(2,1)}, u32[]{:S(2)}) copy-start(bf16[1,2048,256]{2,1,0:T(8,128)(2,1)} %param.31) | copy-start | bytes 3145732
  6.5 3.5 %copy-start.7 = (bf16[512,256]{1,0:T(8,128)(2,1)S(1)}, bf16[512,256]{1,0:T(8,128)(2,1)}, u32[]{:S(2)}) copy-start(bf16[512,256]{1,0:T(8,128)(2,1)} %q_ref.1) | copy-start | bytes 786436
  6.5 3.5 %copy-start.8 = (bf16[512,256]{1,0:T(8,128)(2,1)S(1)}, bf16[512,256]{1,0:T(8,128)(2,1)}, u32[]{:S(2)}) copy-start(bf16[512,256]{1,0:T(8,128)(2,1)} %ff_ref.1) | copy-start | bytes 786436
  6.6 3.5 %copy-start.9 = (bf16[512,256]{1,0:T(8,128)(2,1)S(1)}, bf16[512,256]{1,0:T(8,128)(2,1)}, u32[]{:S(2)}) copy-start(bf16[512,256]{1,0:T(8,128)(2,1)} %fb_ref.1) | copy-start | bytes 786436
  10.1 1.0 copy-start.10
  11.0 0.9 copy-start.11
  90.5 2.8 %copy-start.4 = (bf16[512,256]{1,0:T(8,128)(2,1)}, bf16[512,256]{1,0:T(8,128)(2,1)S(1)}, u32[]{:S(2)}) copy-start(bf16[512,256]{1,0:T(8,128)(2,1)S(1)} %get-tuple-element.13) | copy-start | bytes 786436
  90.5 2.8 %copy-start.16 = (bf16[8,64,2048]{2,1,0:T(8,128)(2,1)S(1)}, bf16[8,64,2048]{2,1,0:T(8,128)(2,1)}, u32[]{:S(2)}) copy-start(bf16[8,64,2048]{2,1,0:T(8,128)(2,1)} %get-tuple-element.9) | copy-start | bytes 6291460
  90.5 3.6 %copy-start.20 = (bf16[3,2048,256]{2,1,0:T(8,128)(2,1)S(1)}, bf16[3,2048,256]{2,1,0:T(8,128)(2,1)}, u32[]{:S(2)}) copy-start(bf16[3,2048,256]{2,1,0:T(8,128)(2,1)} %get-tuple-element.11) | copy-start | bytes 9437188
  94.1 1.9 %copy-start.19 = (bf16[3,2048,256]{2,1,0:T(8,128)(2,1)S(1)}, bf16[3,2048,256]{2,1,0:T(8,128)(2,1)}, u32[]{:S(2)}) copy-start(bf16[3,2048,256]{2,1,0:T(8,128)(2,1)} %get-tuple-element.10) | copy-start | bytes 9437188
  98.2 1.9 %copy-start.18 = (bf16[3,256,2048]{2,1,0:T(8,128)(2,1)S(1)}, bf16[3,256,2048]{2,1,0:T(8,128)(2,1)}, u32[]{:S(2)}) copy-start(bf16[3,256,2048]{2,1,0:T(8,128)(2,1)} %get-tuple-element.12) | copy-start | bytes 9437188
  105.3 6.7 %copy-start.5 = (bf16[512,256]{1,0:T(8,128)(2,1)S(1)}, bf16[512,256]{1,0:T(8,128)(2,1)}, u32[]{:S(2)}) copy-start(bf16[512,256]{1,0:T(8,128)(2,1)} %copy-done.4) | copy-start | bytes 786436
  112.0 1.6 copy-start.1
  162.8 1.4 copy-start.15
  164.1 1.3 copy-start.17
